TPU v7x, 512 devices: a whole 4x8x8 slice. The times are simulated.
512 devices in a mesh: rep: 2 (over z_hi), fs: 32 (over z_lo, y), tp: 8 (over x, core).
Axes of the slice: x: 4, y: 8, z: 8 (z_hi: 2, z_lo: 4; z = z_hi * 4 + z_lo), core: 2. Of those that a mesh axis runs over, the one named last changes fastest.
Arguments:
- x_early: bfloat16 [7168, 2048], P(('rep', 'fs')), may hold values from -6 to 6
- x_late: bfloat16 [7168, 2048], P(('rep', 'fs')), may hold values from -6 to 6
- grad_out: bfloat16 [7168, 2048], P(('rep', 'fs')), may hold values from -16 to 16
- w_gate: bfloat16 [2048, 3072], P('fs', 'tp'), may hold values from -0.125 to 0.125
- w_up: bfloat16 [2048, 3072], P('fs', 'tp'), may hold values from -0.125 to 0.125
- w_down: bfloat16 [3072, 2048], P('tp', 'fs'), may hold values from -0.109375 to 0.109375
- gate_sum: float32 [2048, 3072], P('fs', 'tp'), may hold values from -160 to 160
- up_sum: float32 [2048, 3072], P('fs', 'tp'), may hold values from -160 to 160
- down_sum: float32 [3072, 2048], P('tp', 'fs'), may hold values from -160 to 160
Outputs:
- out_late: bfloat16 [7168, 2048], P(('rep', 'fs'))
- grad_in: bfloat16 [7168, 2048], P(('rep', 'fs'))
- new_gate_sum: float32 [2048, 3072], P('fs', 'tp')
- new_up_sum: float32 [2048, 3072], P('fs', 'tp')
- new_down_sum: float32 [3072, 2048], P('tp', 'fs')
All inputs are finite; a program needn't handle non-finite values.
Results may differ from a plain program's by a relative error of at most 0.018.
Values may be sent and summed in bfloat16 or wider, within the bound.
No kernel may reach another device: no remote copies, remote signals or barrier semaphores. Data moves between devices by JAX's collectives and lax.ppermute only.
A program may use at most 64 MiB of HBM per device.

v0:
```python
import jax
import jax.numpy as jnp
from jax import lax
from jax.sharding import PartitionSpec as P

epsilon = 1e-06


def rows_first(arrays, axis, dims):
    turned = [jnp.moveaxis(a, dim, 0) for a, dim in zip(arrays, dims)]
    both = jnp.concatenate([t.reshape(len(t), -1) for t in turned], axis=1)
    whole, at, gathered = (lax.all_gather(both, axis, axis=0, tiled=True), 0, [])
    for t, dim in zip(turned, dims):
        share = whole[:, at : at + t[0].size].reshape(-1, *t.shape[1:])
        gathered.append(jnp.moveaxis(share, 0, dim))
        at += t[0].size
    return tuple(gathered)


def from_everyone(value, axis):
    copies = jnp.broadcast_to(value, (lax.axis_size(axis), *value.shape))
    return lax.all_to_all(copies, axis, split_axis=0, concat_axis=0, tiled=True)


def taken_together(value, axis):
    return from_everyone(value, axis).astype(jnp.float32).sum(axis=0)


def filled_up(lines, length):
    spare = -len(lines) % length
    return jnp.pad(lines, [(0, spare)] + [(0, 0)] * (lines.ndim - 1))


def total_of(value, axis):
    lines = value.reshape(-1, *value.shape[1:][-1:])
    own = lax.psum_scatter(
        filled_up(lines, lax.axis_size(axis)), axis, scatter_dimension=0, tiled=True
    )
    whole = lax.all_gather(own, axis).reshape(-1, *lines.shape[1:])
    return lax.slice_in_dim(whole, 0, len(lines)).reshape(value.shape)


def sent_together(arrays, axis, dim, along):
    both = jnp.concatenate(arrays, axis=along)
    whole, at, gathered = (lax.all_gather(both, axis, axis=dim, tiled=True), 0, [])
    for a in arrays:
        gathered.append(lax.slice_in_dim(whole, at, at + a.shape[along], axis=along))
        at += a.shape[along]
    return tuple(gathered)


def contract_rows(left, right):
    return lax.dot_general(
        left, right, (((0,), (0,)), ((), ())), preferred_element_type=jnp.float32
    )


def contract_cols(left, right):
    return lax.dot_general(
        left, right, (((1,), (1,)), ((), ())), preferred_element_type=jnp.float32
    )


def shards(x_early, x_late, grad_out, w_gate, w_up, w_down, gate_sum, up_sum, down_sum):
    gate_full, up_full, down_full = rows_first((w_gate, w_up, w_down), "fs", (0, 0, 1))
    batch_rows = x_early.shape[0]
    stacked = jnp.concatenate([x_early, x_late], axis=0).astype(jnp.float32)
    row_scale = lax.rsqrt(jnp.mean(stacked * stacked, axis=-1, keepdims=True) + epsilon)
    normed = (stacked * row_scale).astype(jnp.bfloat16)
    gate_pre = jnp.dot(normed, gate_full, preferred_element_type=jnp.float32)
    up_pre = jnp.dot(normed, up_full, preferred_element_type=jnp.float32)
    gate_sig = jax.nn.sigmoid(gate_pre)
    hidden = (gate_pre * gate_sig * up_pre).astype(jnp.bfloat16)
    late_part = jnp.dot(hidden[batch_rows:], down_full, preferred_element_type=jnp.float32).astype(
        jnp.bfloat16
    )
    branch = taken_together(late_part, "tp").astype(jnp.float32)
    out_late = (stacked[batch_rows:] + 0.5 * branch).astype(jnp.bfloat16)
    early_gate = gate_pre[:batch_rows]
    early_upper = up_pre[:batch_rows]
    early_sig = gate_sig[:batch_rows]
    early_hidden = hidden[:batch_rows]
    early_normed = normed[:batch_rows]
    early_scale = row_scale[:batch_rows]
    grad_hidden = 0.5 * contract_cols(grad_out, down_full)
    grad_gate_in = (
        grad_hidden * early_upper * early_sig * (1.0 + early_gate * (1.0 - early_sig))
    ).astype(jnp.bfloat16)
    grad_up_in = (grad_hidden * early_gate * early_sig).astype(jnp.bfloat16)
    normed_part = contract_cols(grad_gate_in, gate_full) + contract_cols(grad_up_in, up_full)
    grad_normed = total_of(normed_part.astype(jnp.bfloat16), "tp").astype(jnp.float32)
    unit_rows = stacked[:batch_rows] * early_scale
    inner = jnp.mean(grad_normed * unit_rows, axis=-1, keepdims=True)
    grad_in = (
        grad_out.astype(jnp.float32) + early_scale * (grad_normed - unit_rows * inner)
    ).astype(jnp.bfloat16)
    normed_cols, out_cols = (
        lax.all_to_all(early_normed, "fs", split_axis=1, concat_axis=0, tiled=True),
        lax.all_to_all(grad_out, "fs", split_axis=1, concat_axis=0, tiled=True),
    )
    pieces = sent_together((grad_gate_in, grad_up_in, early_hidden), "fs", 0, 1)
    gate_delta = contract_rows(normed_cols, pieces[0])
    up_delta = contract_rows(normed_cols, pieces[1])
    down_half = contract_rows(pieces[2], out_cols)
    down_delta = 0.5 * down_half
    gate_delta, up_delta, down_delta = (
        taken_together(gate_delta.astype(jnp.bfloat16), "rep").astype(jnp.float32),
        taken_together(up_delta.astype(jnp.bfloat16), "rep").astype(jnp.float32),
        taken_together(down_delta.astype(jnp.bfloat16), "rep").astype(jnp.float32),
    )
    return (out_late, grad_in, gate_sum + gate_delta, up_sum + up_delta, down_sum + down_delta)


def solution(mesh):
    placed = (
        P(("rep", "fs"), None),
        P(("rep", "fs"), None),
        P(("rep", "fs"), None),
        P("fs", "tp"),
        P("fs", "tp"),
        P("tp", "fs"),
        P("fs", "tp"),
        P("fs", "tp"),
        P("tp", "fs"),
    )
    return jax.shard_map(
        shards,
        mesh=mesh,
        in_specs=placed,
        out_specs=(
            P(("rep", "fs"), None),
            P(("rep", "fs"), None),
            P("fs", "tp"),
            P("fs", "tp"),
            P("tp", "fs"),
        ),
        check_vma=False,
    )
```

profile of v0, /device:TPU:2, one launch (start us, length us, event | category | flops | bytes accessed | tf_op | source)
XLA Modules:
  0.0 403.2 jit_solution(4803687750171344934)
XLA Ops:
  7.2 1.5 pad_maximum_fusion.1
  8.8 1.4 multiply_reduce_fusion
  10.2 1.4 multiply_convert_fusion
  11.6 163.6 %all-gather.5.cloned.1.call-done = bf16[2048,1152]{1,0:T(8,128)(2,1)} async-done(((bf16[64,1152]{1,0:T(8,128)(2,1)}), bf16[2048,1152]{1,0:T(8,128)(2,1)}) %all-gather.5.cloned.1.call-update) | async-done | bytes 4718608 | tf_op jit(solution)/shard_map/all_gather | solution.py:12
  175.2 2.0 fusion.12
  177.2 2.1 add_divide_fusion
  179.4 1.9 multiply_convert_fusion.2
  181.3 0.7 pad_maximum_fusion
  182.1 1.0 copy.24
  183.1 9.5 %all-to-all-start.1 = ((bf16[112,32,64]{0,2,1:T(8,128)(2,1)}), bf16[112,32,64]{0,2,1:T(8,128)(2,1)S(1)}, u32[]{:S(2)}, u32[]{:S(2)}) async-start(bf16[112,32,64]{0,2,1:T(8,128)(2,1)} %bitcast.3), calls=%async_computation.1 | async-start | bytes 1048576 | tf_op jit(solution)/shard_map/all_to_all | solution.py:98
  192.6 1.0 copy.26
  193.6 16.0 %all-to-all-done.1 = bf16[112,32,64]{0,2,1:T(8,128)(2,1)S(1)} async-done(((bf16[112,32,64]{0,2,1:T(8,128)(2,1)}), bf16[112,32,64]{0,2,1:T(8,128)(2,1)S(1)}, u32[]{:S(2)}, u32[]{:S(2)}) %all-to-all-start.1) | async-done | bytes 458784 | tf_op jit(solution)/shard_map/all_to_all | solution.py:98
  209.6 6.4 %all-to-all-start.4 = ((bf16[112,32,64]{0,2,1:T(8,128)(2,1)}), bf16[112,32,64]{0,2,1:T(8,128)(2,1)S(1)}, u32[]{:S(2)}, u32[]{:S(2)}) async-start(bf16[112,32,64]{0,2,1:T(8,128)(2,1)} %bitcast.5), calls=%async_computation.4 | async-start | bytes 1048576 | tf_op jit(solution)/shard_map/all_to_all | solution.py:99
  216.1 2.0 convolution_convert_fusion
  218.1 15.3 %all-to-all-done.4 = bf16[112,32,64]{0,2,1:T(8,128)(2,1)S(1)} async-done(((bf16[112,32,64]{0,2,1:T(8,128)(2,1)}), bf16[112,32,64]{0,2,1:T(8,128)(2,1)S(1)}, u32[]{:S(2)}, u32[]{:S(2)}) %all-to-all-start.4) | async-done | bytes 458784 | tf_op jit(solution)/shard_map/all_to_all | solution.py:99
  233.4 2.3 broadcast_in_dim.14
  235.6 5.0 %all-to-all-start = ((bf16[8,112,2048]{2,1,0:T(8,128)(2,1)}), bf16[8,112,2048]{2,1,0:T(8,128)(2,1)}, u32[]{:S(2)}, u32[]{:S(2)}) async-start(bf16[8,112,2048]{2,1,0:T(8,128)(2,1)} %broadcast_in_dim.14), calls=%async_computation | async-start | bytes 7340032 | tf_op jit(solution)/shard_map/all_to_all | solution.py:22
  240.6 2.1 fusion.14
  242.7 2.0 fusion.7
  244.7 47.1 %fusion = bf16[16,2048]{1,0:T(8,128)(2,1)S(1)} fusion(bf16[112,2048]{1,0:T(8,128)(2,1)S(1)} %fusion.7), kind=kCustom, calls=%all-reduce-scatter | all-reduce-scatter fusion | flops 262145 | bytes 526336
  291.9 1.9 collective-permute-start
  293.8 0.2 maximum_convert_fusion
  294.0 1.3 dynamic-slice.4
  296.0 0.3 copy.25
  296.3 1.8 all_to_all.44
  298.1 1.4 copy.27
  299.5 1.8 all_to_all.50
  301.2 0.2 concatenate.12
  301.5 13.2 %all-gather.1 = bf16[8,14,2048]{2,1,0:T(8,128)(2,1)S(1)} all-gather(bf16[1,14,2048]{2,1,0:T(8,128)(2,1)S(1)} %dynamic-slice_bitcast_fusion), channel_id=2, replica_groups=mesh['rep'=2,'fs'=32,'tp'=8] {'tp'}, dimensions={0}, use_global_device_ids=true | all-gather | bytes 516096 | tf_op jit(solution)/shard_map/all_gather | solution.py:39
  314.8 0.2 multiply_reduce_fusion.1
  315.1 2.9 convert_reduce_fusion
  317.9 1.2 add_convert_fusion
  319.1 37.0 %all-gather.7.cloned.1.call-done = bf16[3584,1152]{1,0:T(8,128)(2,1)} async-done(((bf16[112,1152]{1,0:T(8,128)(2,1)}), bf16[3584,1152]{1,0:T(8,128)(2,1)}) %all-gather.7.cloned.1.call-update) | async-done | bytes 8257552 | tf_op jit(solution)/shard_map/all_gather | solution.py:45
  356.2 2.5 fusion.30
  358.7 0.7 broadcast_in_dim.15
  359.3 3.4 all-to-all-start.2
  362.7 2.3 fusion.33
  365.1 2.4 fusion.27
  367.4 3.5 all-to-all-done.2
  370.9 0.6 broadcast_in_dim.16
  371.5 3.8 all-to-all-start.3
  375.3 0.7 add.49
  376.0 7.5 %all-to-all-done.3 = bf16[2,64,384]{2,1,0:T(8,128)(2,1)S(1)} async-done(((bf16[2,64,384]{2,1,0:T(8,128)(2,1)}), bf16[2,64,384]{2,1,0:T(8,128)(2,1)S(1)}, u32[]{:S(2)}, u32[]{:S(2)}) %all-to-all-start.3) | async-done | bytes 98336 | tf_op jit(solution)/shard_map/all_to_all | solution.py:22
  383.5 0.6 broadcast_in_dim.17
  384.1 3.3 all-to-all-start.5
  387.5 0.7 add.50
  388.2 7.5 %all-to-all-done.5 = bf16[2,384,64]{1,2,0:T(8,128)(2,1)S(1)} async-done(((bf16[2,384,64]{1,2,0:T(8,128)(2,1)}), bf16[2,384,64]{1,2,0:T(8,128)(2,1)S(1)}, u32[]{:S(2)}, u32[]{:S(2)}) %all-to-all-start.5) | async-done | bytes 98336 | tf_op jit(solution)/shard_map/all_to_all | solution.py:22
  395.7 0.7 add.51
  (37 shorter events, 0.4 us)
Async XLA Ops:
  7.2 168.0 %all-gather.5.cloned.1.call-start = ((), (), s32[]{:S(2)}) async-start(), calls=%async_computation.6 | async-start | bytes 4866048 | tf_op jit(solution)/shard_map/all_gather | solution.py:12
  8.8 347.4 %all-gather.7.cloned.1.call-start = ((), (), s32[]{:S(2)}) async-start(), calls=%async_computation.7 | async-start | bytes 8515584 | tf_op jit(solution)/shard_map/all_gather | solution.py:45
  177.2 2.2 copy-start.3
  183.1 26.5 %all-to-all-start.1 = ((bf16[112,32,64]{0,2,1:T(8,128)(2,1)}), bf16[112,32,64]{0,2,1:T(8,128)(2,1)S(1)}, u32[]{:S(2)}, u32[]{:S(2)}) async-start(bf16[112,32,64]{0,2,1:T(8,128)(2,1)} %bitcast.3), calls=%async_computation.1 | async-start | bytes 1048576 | tf_op jit(solution)/shard_map/all_to_all | solution.py:98
  209.6 23.8 %all-to-all-start.4 = ((bf16[112,32,64]{0,2,1:T(8,128)(2,1)}), bf16[112,32,64]{0,2,1:T(8,128)(2,1)S(1)}, u32[]{:S(2)}, u32[]{:S(2)}) async-start(bf16[112,32,64]{0,2,1:T(8,128)(2,1)} %bitcast.5), calls=%async_computation.4 | async-start | bytes 1048576 | tf_op jit(solution)/shard_map/all_to_all | solution.py:99
  233.4 2.3 copy-start.2
  235.6 79.4 %all-to-all-start = ((bf16[8,112,2048]{2,1,0:T(8,128)(2,1)}), bf16[8,112,2048]{2,1,0:T(8,128)(2,1)}, u32[]{:S(2)}, u32[]{:S(2)}) async-start(bf16[8,112,2048]{2,1,0:T(8,128)(2,1)} %broadcast_in_dim.14), calls=%async_computation | async-start | bytes 7340032 | tf_op jit(solution)/shard_map/all_to_all | solution.py:22
  240.6 53.2 %copy-start = (bf16[112,2048]{1,0:T(8,128)(2,1)S(1)}, bf16[112,2048]{1,0:T(8,128)(2,1)}, u32[]{:S(2)}) copy-start(bf16[112,2048]{1,0:T(8,128)(2,1)} %param.10) | copy-start | bytes 1376260
  240.6 53.2 %copy-start.1 = (bf16[112,2048]{1,0:T(8,128)(2,1)S(1)}, bf16[112,2048]{1,0:T(8,128)(2,1)}, u32[]{:S(2)}) copy-start(bf16[112,2048]{1,0:T(8,128)(2,1)} %param.9) | copy-start | bytes 1376260
  291.9 9.4 %collective-permute-start = (bf16[14,2048]{1,0:T(8,128)(2,1)S(1)}, bf16[14,2048]{1,0:T(8,128)(2,1)S(1)}, u32[]{:S(2)}, u32[]{:S(2)}) collective-permute-start(bf16[14,2048]{1,0:T(8,128)(2,1)S(1)} %slice.75), channel_id=1, source_target_pairs={{0,1},{1,2},{2,3},{3,4},{4,5},{5,6},{6,7},{8,9},{9,10},{10,11},{11... | collective-permute-start | bytes 172040
  315.0 2.9 copy-start.4
  319.1 43.5 %copy-start.5 = (bf16[3584,64]{0,1:T(8,128)(2,1)S(1)}, bf16[3584,64]{0,1:T(8,128)(2,1)}, u32[]{:S(2)}) copy-start(bf16[3584,64]{0,1:T(8,128)(2,1)} %all_to_all.44) | copy-start | bytes 1376260
  358.7 6.4 %copy-start.6 = (bf16[3584,64]{0,1:T(8,128)(2,1)S(1)}, bf16[3584,64]{0,1:T(8,128)(2,1)}, u32[]{:S(2)}) copy-start(bf16[3584,64]{0,1:T(8,128)(2,1)} %all_to_all.50) | copy-start | bytes 1376260
  359.3 11.6 %all-to-all-start.2 = ((bf16[2,64,384]{2,1,0:T(8,128)(2,1)}), bf16[2,64,384]{2,1,0:T(8,128)(2,1)S(1)}, u32[]{:S(2)}, u32[]{:S(2)}) async-start(bf16[2,64,384]{2,1,0:T(8,128)(2,1)} %broadcast_in_dim.15), calls=%async_computation.2 | async-start | bytes 196608 | tf_op jit(solution)/shard_map/all_to_all | solution.py:22
  365.0 10.3 %copy-start.7 = (f32[64,384]{1,0:T(8,128)S(1)}, f32[64,384]{1,0:T(8,128)}, u32[]{:S(2)}) copy-start(f32[64,384]{1,0:T(8,128)} %param.15) | copy-start | bytes 294916
  365.0 22.5 %copy-start.8 = (f32[64,384]{1,0:T(8,128)S(1)}, f32[64,384]{1,0:T(8,128)}, u32[]{:S(2)}) copy-start(f32[64,384]{1,0:T(8,128)} %param.16) | copy-start | bytes 294916
  365.0 30.7 %copy-start.9 = (f32[384,64]{0,1:T(8,128)S(1)}, f32[384,64]{0,1:T(8,128)}, u32[]{:S(2)}) copy-start(f32[384,64]{0,1:T(8,128)} %param.17) | copy-start | bytes 294916
  371.5 12.0 %all-to-all-start.3 = ((bf16[2,64,384]{2,1,0:T(8,128)(2,1)}), bf16[2,64,384]{2,1,0:T(8,128)(2,1)S(1)}, u32[]{:S(2)}, u32[]{:S(2)}) async-start(bf16[2,64,384]{2,1,0:T(8,128)(2,1)} %broadcast_in_dim.16), calls=%async_computation.3 | async-start | bytes 196608 | tf_op jit(solution)/shard_map/all_to_all | solution.py:22
  384.1 11.5 %all-to-all-start.5 = ((bf16[2,384,64]{1,2,0:T(8,128)(2,1)}), bf16[2,384,64]{1,2,0:T(8,128)(2,1)S(1)}, u32[]{:S(2)}, u32[]{:S(2)}) async-start(bf16[2,384,64]{1,2,0:T(8,128)(2,1)} %broadcast_in_dim.17), calls=%async_computation.5 | async-start | bytes 196608 | tf_op jit(solution)/shard_map/all_to_all | solution.py:22
Sparse Core Ops, SparseCore 0:
  10.6 164.5 all-gather.4
  182.1 173.9 all-gather.6
where the time goes:
time: 404 us; the launch traced here: 403 us
  waiting for transfers between devices  250 us (62%)
  blocking collectives  60.3 us (15%)
  starting transfers between devices  33.4 us (8%)
  matrix products  19.3 us (5%)
  between operations  15 us (4%)
  local copies, waits for them, and re-layouts  13.2 us (3%)
  other arithmetic  11.6 us (3%)
    all_gather x1, waiting for transfers between devices, rows_first(): lax.all_gather(both, axis, axis=0, tiled=True)  164 us
    unnamed x1, blocking collectives  47.1 us
    all_gather x1, waiting for transfers between devices, sent_together(): lax.all_gather(both, axis, axis=dim, tiled=True)  37 us
    all_to_all x4, waiting for transfers between devices, from_everyone(): return lax.all_to_all(copies, axis, split_axis=0, concat_axis=0, tiled=True)  18.5 us
    all_to_all x1, waiting for transfers between devices, shards(): lax.all_to_all(early_normed, 'fs', split_axis=1, concat_axis=0, tiled=True)  16 us
    all_to_all x4, starting transfers between devices, from_everyone(): return lax.all_to_all(copies, axis, split_axis=0, concat_axis=0, tiled=True)  15.4 us
    all_to_all x1, waiting for transfers between devices, shards(): lax.all_to_all(grad_out, 'fs', split_axis=1, concat_axis=0, tiled=True)  15.3 us
    all_gather x1, blocking collectives, total_of(): whole = lax.all_gather(own, axis).reshape(-1, *lines.shape[1:])  13.2 us
  transfers between devices with their start and end apart: 9, of which 7 were waited for; matrix products, arithmetic and copies ran while one was open for 18% of the time, Pallas kernels for 0%

commit v1 on v0

--- a/solution.py
+++ b/solution.py
@@ -4,12 +4,21 @@
 from jax.sharding import PartitionSpec as P
 
 epsilon = 1e-06
+start_edges = lambda z_in, axis_name, d0: jnp.concatenate(
+    lax.all_to_all(
+        jnp.stack([z_in for _ in range(lax.axis_size(axis_name))]),
+        axis_name=axis_name,
+        split_axis=0,
+        concat_axis=0,
+    ),
+    d0,
+)
 
 
 def rows_first(arrays, axis, dims):
     turned = [jnp.moveaxis(a, dim, 0) for a, dim in zip(arrays, dims)]
     both = jnp.concatenate([t.reshape(len(t), -1) for t in turned], axis=1)
-    whole, at, gathered = (lax.all_gather(both, axis, axis=0, tiled=True), 0, [])
+    whole, at, gathered = (start_edges(both, axis, 0), 0, [])
     for t, dim in zip(turned, dims):
         share = whole[:, at : at + t[0].size].reshape(-1, *t.shape[1:])
         gathered.append(jnp.moveaxis(share, 0, dim))

time: 404 us -> 388 us (0.960)
  the two profiles are of different devices: /device:TPU:2 before, /device:TPU:6 now
where the time goes in v1:
time: 388 us; the launch traced here: 387 us
  waiting for transfers between devices  216 us (56%)
  blocking collectives  60.3 us (16%)
  starting transfers between devices  51.8 us (13%)
  matrix products  19.3 us (5%)
  local copies, waits for them, and re-layouts  16 us (4%)
  between operations  15 us (4%)
  other arithmetic  8.59 us (2%)
    all_to_all x1, waiting for transfers between devices, lax.all_to_all(jnp.stack([z_in for _ in range(lax.axis_size(axis_name))])...  120 us
    unnamed x1, blocking collectives  47.2 us
    all_gather x1, waiting for transfers between devices, sent_together(): lax.all_gather(both, axis, axis=dim, tiled=True)  38.8 us
    all_to_all x1, waiting for transfers between devices, shards(): lax.all_to_all(grad_out, 'fs', split_axis=1, concat_axis=0, tiled=True)  19.2 us
    all_to_all x1, waiting for transfers between devices, shards(): lax.all_to_all(early_normed, 'fs', split_axis=1, concat_axis=0, tiled=True)  19.2 us
    all_to_all x4, starting transfers between devices, from_everyone(): return lax.all_to_all(copies, axis, split_axis=0, concat_axis=0, tiled=True)  19.1 us
    all_to_all x4, waiting for transfers between devices, from_everyone(): return lax.all_to_all(copies, axis, split_axis=0, concat_axis=0, tiled=True)  18.5 us
    all_to_all x1, starting transfers between devices, lax.all_to_all(jnp.stack([z_in for _ in range(lax.axis_size(axis_name))])...  13.2 us
  transfers between devices with their start and end apart: 9, of which 7 were waited for; matrix products, arithmetic and copies ran while one was open for 19% of the time, Pallas kernels for 0%

profile of v1, /device:TPU:6, one launch (start us, length us, event | category | flops | bytes accessed | tf_op | source)
XLA Modules:
  0.0 387.0 jit_solution(5191975285264908568)
XLA Ops:
  7.2 0.9 pad_maximum_fusion.1
  8.0 2.8 stack.2
  10.8 13.2 %all-to-all-start = ((bf16[32,64,1152]{2,1,0:T(8,128)(2,1)}), bf16[32,64,1152]{2,1,0:T(8,128)(2,1)}, u32[]{:S(2)}, u32[]{:S(2)}) async-start(bf16[32,64,1152]{2,1,0:T(8,128)(2,1)} %stack.2), calls=%async_computation | async-start | bytes 9437184 | tf_op jit(solution)/shard_map/all_to_all | solution.py:8
  24.1 0.3 multiply_reduce_fusion
  24.3 0.2 multiply_convert_fusion
  24.6 120.3 %all-to-all-done = bf16[32,64,1152]{2,1,0:T(8,128)(2,1)} async-done(((bf16[32,64,1152]{2,1,0:T(8,128)(2,1)}), bf16[32,64,1152]{2,1,0:T(8,128)(2,1)}, u32[]{:S(2)}, u32[]{:S(2)}) %all-to-all-start) | async-done | bytes 4718624 | tf_op jit(solution)/shard_map/all_to_all | solution.py:8
  144.9 2.0 fusion.12
  146.9 2.1 add_divide_fusion
  149.1 1.9 multiply_convert_fusion.2
  151.0 0.7 pad_maximum_fusion
  151.7 1.0 copy.24
  152.8 12.5 %all-to-all-start.2 = ((bf16[112,32,64]{0,2,1:T(8,128)(2,1)}), bf16[112,32,64]{0,2,1:T(8,128)(2,1)S(1)}, u32[]{:S(2)}, u32[]{:S(2)}) async-start(bf16[112,32,64]{0,2,1:T(8,128)(2,1)} %bitcast.4), calls=%async_computation.2 | async-start | bytes 1048576 | tf_op jit(solution)/shard_map/all_to_all | solution.py:107
  165.3 1.0 copy.26
  166.3 19.2 %all-to-all-done.2 = bf16[112,32,64]{0,2,1:T(8,128)(2,1)S(1)} async-done(((bf16[112,32,64]{0,2,1:T(8,128)(2,1)}), bf16[112,32,64]{0,2,1:T(8,128)(2,1)S(1)}, u32[]{:S(2)}, u32[]{:S(2)}) %all-to-all-start.2) | async-done | bytes 458784 | tf_op jit(solution)/shard_map/all_to_all | solution.py:107
  185.5 5.1 %all-to-all-start.5 = ((bf16[112,32,64]{0,2,1:T(8,128)(2,1)}), bf16[112,32,64]{0,2,1:T(8,128)(2,1)S(1)}, u32[]{:S(2)}, u32[]{:S(2)}) async-start(bf16[112,32,64]{0,2,1:T(8,128)(2,1)} %bitcast.6), calls=%async_computation.5 | async-start | bytes 1048576 | tf_op jit(solution)/shard_map/all_to_all | solution.py:108
  190.6 2.0 convolution_convert_fusion
  192.6 19.2 %all-to-all-done.5 = bf16[112,32,64]{0,2,1:T(8,128)(2,1)S(1)} async-done(((bf16[112,32,64]{0,2,1:T(8,128)(2,1)}), bf16[112,32,64]{0,2,1:T(8,128)(2,1)S(1)}, u32[]{:S(2)}, u32[]{:S(2)}) %all-to-all-start.5) | async-done | bytes 458784 | tf_op jit(solution)/shard_map/all_to_all | solution.py:108
  211.8 2.3 broadcast_in_dim.14
  214.1 5.1 %all-to-all-start.1 = ((bf16[8,112,2048]{2,1,0:T(8,128)(2,1)}), bf16[8,112,2048]{2,1,0:T(8,128)(2,1)}, u32[]{:S(2)}, u32[]{:S(2)}) async-start(bf16[8,112,2048]{2,1,0:T(8,128)(2,1)} %broadcast_in_dim.14), calls=%async_computation.1 | async-start | bytes 7340032 | tf_op jit(solution)/shard_map/all_to_all | solution.py:31
  219.2 2.0 fusion.14
  221.3 2.0 fusion.7
  223.3 47.2 %fusion = bf16[16,2048]{1,0:T(8,128)(2,1)S(1)} fusion(bf16[112,2048]{1,0:T(8,128)(2,1)S(1)} %fusion.7), kind=kCustom, calls=%all-reduce-scatter | all-reduce-scatter fusion | flops 262145 | bytes 526336
  270.5 1.9 collective-permute-start
  272.7 1.3 dynamic-slice.4
  274.6 0.3 copy.25
  275.0 1.8 all_to_all.48
  276.7 1.4 copy.27
  278.1 1.8 all_to_all.54
  280.1 13.1 %all-gather.1 = bf16[8,14,2048]{2,1,0:T(8,128)(2,1)S(1)} all-gather(bf16[1,14,2048]{2,1,0:T(8,128)(2,1)S(1)} %dynamic-slice_bitcast_fusion), channel_id=2, replica_groups=mesh['rep'=2,'fs'=32,'tp'=8] {'tp'}, dimensions={0}, use_global_device_ids=true | all-gather | bytes 516096 | tf_op jit(solution)/shard_map/all_gather | solution.py:48
  293.4 0.2 multiply_reduce_fusion.1
  293.6 2.9 convert_reduce_fusion
  296.5 1.2 add_convert_fusion
  297.7 38.8 %all-gather.4.cloned.1.call-done = bf16[3584,1152]{1,0:T(8,128)(2,1)} async-done(((bf16[112,1152]{1,0:T(8,128)(2,1)}), bf16[3584,1152]{1,0:T(8,128)(2,1)}) %all-gather.4.cloned.1.call-update) | async-done | bytes 8257552 | tf_op jit(solution)/shard_map/all_gather | solution.py:54
  336.5 2.5 fusion.30
  339.0 0.7 broadcast_in_dim.15
  339.7 6.8 %all-to-all-start.3 = ((bf16[2,64,384]{2,1,0:T(8,128)(2,1)}), bf16[2,64,384]{2,1,0:T(8,128)(2,1)S(1)}, u32[]{:S(2)}, u32[]{:S(2)}) async-start(bf16[2,64,384]{2,1,0:T(8,128)(2,1)} %broadcast_in_dim.15), calls=%async_computation.3 | async-start | bytes 196608 | tf_op jit(solution)/shard_map/all_to_all | solution.py:31
  346.5 2.3 fusion.33
  348.9 2.4 fusion.27
  351.2 3.5 all-to-all-done.3
  354.7 0.6 broadcast_in_dim.16
  355.3 3.8 all-to-all-start.4
  359.1 0.7 add.49
  359.8 7.5 %all-to-all-done.4 = bf16[2,64,384]{2,1,0:T(8,128)(2,1)S(1)} async-done(((bf16[2,64,384]{2,1,0:T(8,128)(2,1)}), bf16[2,64,384]{2,1,0:T(8,128)(2,1)S(1)}, u32[]{:S(2)}, u32[]{:S(2)}) %all-to-all-start.4) | async-done | bytes 98336 | tf_op jit(solution)/shard_map/all_to_all | solution.py:31
  367.3 0.6 broadcast_in_dim.17
  368.0 3.3 all-to-all-start.6
  371.3 0.7 add.50
  372.0 7.5 %all-to-all-done.6 = bf16[2,384,64]{1,2,0:T(8,128)(2,1)S(1)} async-done(((bf16[2,384,64]{1,2,0:T(8,128)(2,1)}), bf16[2,384,64]{1,2,0:T(8,128)(2,1)S(1)}, u32[]{:S(2)}, u32[]{:S(2)}) %all-to-all-start.6) | async-done | bytes 98336 | tf_op jit(solution)/shard_map/all_to_all | solution.py:31
  379.5 0.7 add.51
  (37 shorter events, 0.8 us)
Async XLA Ops:
  10.8 13.2 %copy-start = (bf16[112,2048]{1,0:T(8,128)(2,1)S(1)}, bf16[112,2048]{1,0:T(8,128)(2,1)}, u32[]{:S(2)}) copy-start(bf16[112,2048]{1,0:T(8,128)(2,1)} %param.10) | copy-start | bytes 1376260
  10.8 13.2 %copy-start.1 = (bf16[112,2048]{1,0:T(8,128)(2,1)S(1)}, bf16[112,2048]{1,0:T(8,128)(2,1)}, u32[]{:S(2)}) copy-start(bf16[112,2048]{1,0:T(8,128)(2,1)} %param.9) | copy-start | bytes 1376260
  10.8 134.0 %all-to-all-start = ((bf16[32,64,1152]{2,1,0:T(8,128)(2,1)}), bf16[32,64,1152]{2,1,0:T(8,128)(2,1)}, u32[]{:S(2)}, u32[]{:S(2)}) async-start(bf16[32,64,1152]{2,1,0:T(8,128)(2,1)} %stack.2), calls=%async_computation | async-start | bytes 9437184 | tf_op jit(solution)/shard_map/all_to_all | solution.py:8
  24.0 312.5 %all-gather.4.cloned.1.call-start = ((), (), s32[]{:S(2)}) async-start(), calls=%async_computation.7 | async-start | bytes 8515584 | tf_op jit(solution)/shard_map/all_gather | solution.py:54
  146.9 2.2 copy-start.3
  152.8 32.7 %all-to-all-start.2 = ((bf16[112,32,64]{0,2,1:T(8,128)(2,1)}), bf16[112,32,64]{0,2,1:T(8,128)(2,1)S(1)}, u32[]{:S(2)}, u32[]{:S(2)}) async-start(bf16[112,32,64]{0,2,1:T(8,128)(2,1)} %bitcast.4), calls=%async_computation.2 | async-start | bytes 1048576 | tf_op jit(solution)/shard_map/all_to_all | solution.py:107
  185.5 26.4 %all-to-all-start.5 = ((bf16[112,32,64]{0,2,1:T(8,128)(2,1)}), bf16[112,32,64]{0,2,1:T(8,128)(2,1)S(1)}, u32[]{:S(2)}, u32[]{:S(2)}) async-start(bf16[112,32,64]{0,2,1:T(8,128)(2,1)} %bitcast.6), calls=%async_computation.5 | async-start | bytes 1048576 | tf_op jit(solution)/shard_map/all_to_all | solution.py:108
  211.8 2.3 copy-start.2
  214.1 79.5 %all-to-all-start.1 = ((bf16[8,112,2048]{2,1,0:T(8,128)(2,1)}), bf16[8,112,2048]{2,1,0:T(8,128)(2,1)}, u32[]{:S(2)}, u32[]{:S(2)}) async-start(bf16[8,112,2048]{2,1,0:T(8,128)(2,1)} %broadcast_in_dim.14), calls=%async_computation.1 | async-start | bytes 7340032 | tf_op jit(solution)/shard_map/all_to_all | solution.py:31
  270.5 9.4 %collective-permute-start = (bf16[14,2048]{1,0:T(8,128)(2,1)S(1)}, bf16[14,2048]{1,0:T(8,128)(2,1)S(1)}, u32[]{:S(2)}, u32[]{:S(2)}) collective-permute-start(bf16[14,2048]{1,0:T(8,128)(2,1)S(1)} %slice.75), channel_id=1, source_target_pairs={{0,1},{1,2},{2,3},{3,4},{4,5},{5,6},{6,7},{8,9},{9,10},{10,11},{11... | collective-permute-start | bytes 172040
  293.6 2.9 copy-start.4
  297.7 48.8 %copy-start.5 = (bf16[3584,64]{0,1:T(8,128)(2,1)S(1)}, bf16[3584,64]{0,1:T(8,128)(2,1)}, u32[]{:S(2)}) copy-start(bf16[3584,64]{0,1:T(8,128)(2,1)} %all_to_all.48) | copy-start | bytes 1376260
  339.0 9.8 %copy-start.6 = (bf16[3584,64]{0,1:T(8,128)(2,1)S(1)}, bf16[3584,64]{0,1:T(8,128)(2,1)}, u32[]{:S(2)}) copy-start(bf16[3584,64]{0,1:T(8,128)(2,1)} %all_to_all.54) | copy-start | bytes 1376260
  339.7 15.0 %all-to-all-start.3 = ((bf16[2,64,384]{2,1,0:T(8,128)(2,1)}), bf16[2,64,384]{2,1,0:T(8,128)(2,1)S(1)}, u32[]{:S(2)}, u32[]{:S(2)}) async-start(bf16[2,64,384]{2,1,0:T(8,128)(2,1)} %broadcast_in_dim.15), calls=%async_computation.3 | async-start | bytes 196608 | tf_op jit(solution)/shard_map/all_to_all | solution.py:31
  348.8 10.3 %copy-start.7 = (f32[64,384]{1,0:T(8,128)S(1)}, f32[64,384]{1,0:T(8,128)}, u32[]{:S(2)}) copy-start(f32[64,384]{1,0:T(8,128)} %param.15) | copy-start | bytes 294916
  348.8 22.5 %copy-start.8 = (f32[64,384]{1,0:T(8,128)S(1)}, f32[64,384]{1,0:T(8,128)}, u32[]{:S(2)}) copy-start(f32[64,384]{1,0:T(8,128)} %param.16) | copy-start | bytes 294916
  348.9 30.7 %copy-start.9 = (f32[384,64]{0,1:T(8,128)S(1)}, f32[384,64]{0,1:T(8,128)}, u32[]{:S(2)}) copy-start(f32[384,64]{0,1:T(8,128)} %param.17) | copy-start | bytes 294916
  355.3 12.0 %all-to-all-start.4 = ((bf16[2,64,384]{2,1,0:T(8,128)(2,1)}), bf16[2,64,384]{2,1,0:T(8,128)(2,1)S(1)}, u32[]{:S(2)}, u32[]{:S(2)}) async-start(bf16[2,64,384]{2,1,0:T(8,128)(2,1)} %broadcast_in_dim.16), calls=%async_computation.4 | async-start | bytes 196608 | tf_op jit(solution)/shard_map/all_to_all | solution.py:31
  368.0 11.5 %all-to-all-start.6 = ((bf16[2,384,64]{1,2,0:T(8,128)(2,1)}), bf16[2,384,64]{1,2,0:T(8,128)(2,1)S(1)}, u32[]{:S(2)}, u32[]{:S(2)}) async-start(bf16[2,384,64]{1,2,0:T(8,128)(2,1)} %broadcast_in_dim.17), calls=%async_computation.6 | async-start | bytes 196608 | tf_op jit(solution)/shard_map/all_to_all | solution.py:31
Sparse Core Ops, SparseCore 0:
  151.8 184.6 all-gather.3
